TPU v7x, 32 devices: a whole 2x2x4 slice. The times are simulated.
32 devices in a mesh: sp: 4 (over y, x), dp: 8 (over z, core).
Axes of the slice: x: 2, y: 2, z: 4, core: 2. Of those that a mesh axis runs over, the one named last changes fastest.
Arguments:
- value_half: bfloat16 [8, 1024, 2048], P('dp', 'sp'), may hold values from -6 to 6
- gate_half: bfloat16 [8, 1024, 2048], P('dp', 'sp'), may hold values from -6 to 6
- upstream: bfloat16 [8, 1024, 2048], P('dp', 'sp'), may hold values from -6 to 6
- conv_taps: float32 [31, 2048], P(None, 'sp'), may hold values from -1 to 1
- norm_gain: float32 [2048], replicated, may hold values from 0.1 to 1.9
- out_weight: bfloat16 [2048, 2048], P('dp'), may hold values from -0.125 to 0.125
Outputs:
- grad_value: bfloat16 [8, 1024, 2048], P('dp', 'sp')
- grad_gate: bfloat16 [8, 1024, 2048], P('dp', 'sp')
- grad_taps: float32 [31, 2048], P(None, 'sp')
- grad_gain: float32 [2048], replicated
- grad_weight: float32 [2048, 2048], P('dp')
All inputs are finite; a program needn't handle non-finite values.
Results may differ from a plain program's by a relative error of at most 0.0062.
Values may be sent and summed in bfloat16 or wider, within the bound.
A program may use at most 128 MiB of HBM per device.

v0:
```python
import jax
import jax.numpy as jnp
from jax import lax
from jax.sharding import PartitionSpec as P

NORM_EPS = 1e-05


def body(value_half, gate_half, upstream, conv_taps, norm_gain, out_weight):
    tap_count = conv_taps.shape[0]
    sig_gate = jax.nn.sigmoid(gate_half.astype(jnp.float32))
    value_wide = value_half.astype(jnp.float32)
    glu = (value_wide * sig_gate).astype(jnp.bfloat16)
    glu_heads = lax.all_to_all(glu, "sp", split_axis=2, concat_axis=1, tiled=True).astype(
        jnp.float32
    )
    length = glu_heads.shape[1]
    padded = jnp.pad(glu_heads, ((0, 0), (tap_count - 1, 0), (0, 0)))
    conv_out = jnp.zeros_like(glu_heads)
    for offset in range(tap_count):
        conv_out = conv_out + conv_taps[offset] * padded[:, offset : offset + length]
    conv_tokens = lax.all_to_all(
        conv_out.astype(jnp.bfloat16), "sp", split_axis=1, concat_axis=2, tiled=True
    ).astype(jnp.float32)
    row_mean = jnp.mean(conv_tokens, axis=-1, keepdims=True)
    centered = conv_tokens - row_mean
    inv_scale = lax.rsqrt(jnp.mean(centered * centered, axis=-1, keepdims=True) + NORM_EPS)
    normed = centered * inv_scale
    scaled = normed * norm_gain
    sig_scaled = jax.nn.sigmoid(scaled)
    activated = (scaled * sig_scaled).astype(jnp.bfloat16)[0]
    upstream_rows = upstream[0]
    columns = upstream_rows
    grad_act = jnp.dot(
        columns,
        lax.all_gather(out_weight, "dp", axis=0, tiled=True),
        preferred_element_type=jnp.float32,
    )
    grad_scaled = grad_act[None] * sig_scaled * (1.0 + scaled * (1.0 - sig_scaled))
    gain_part = jnp.sum(grad_scaled * normed, axis=(0, 1))
    grad_normed = grad_scaled * norm_gain
    grad_conv_out = inv_scale * (
        grad_normed
        - jnp.mean(grad_normed, axis=-1, keepdims=True)
        - normed * jnp.mean(grad_normed * normed, axis=-1, keepdims=True)
    )
    grad_heads = lax.all_to_all(
        grad_conv_out.astype(jnp.bfloat16), "sp", split_axis=2, concat_axis=1, tiled=True
    ).astype(jnp.float32)
    grad_padded = jnp.pad(grad_heads, ((0, 0), (0, tap_count - 1), (0, 0)))
    grad_glu = jnp.zeros_like(grad_heads)
    tap_terms = []
    for offset in range(tap_count):
        first = tap_count - 1 - offset
        grad_glu = grad_glu + conv_taps[offset] * grad_padded[:, first : first + length]
        tap_terms.append(jnp.sum(grad_heads * padded[:, offset : offset + length], axis=(0, 1)))
    grad_taps = lax.psum(jnp.stack(tap_terms), "dp")
    grad_tokens = lax.all_to_all(
        grad_glu.astype(jnp.bfloat16), "sp", split_axis=1, concat_axis=2, tiled=True
    ).astype(jnp.float32)
    grad_value = (grad_tokens * sig_gate).astype(jnp.bfloat16)
    grad_gate = (grad_tokens * value_wide * sig_gate * (1.0 - sig_gate)).astype(jnp.bfloat16)
    grad_gain = lax.psum(gain_part, ("sp", "dp"))
    columns = upstream_rows
    owned = lax.psum_scatter(
        lax.dot_general(
            columns, activated, (((0,), (0,)), ((), ())), preferred_element_type=jnp.float32
        ),
        "dp",
        scatter_dimension=0,
        tiled=True,
    )
    grad_weight = lax.psum(owned, "sp")
    return (grad_value, grad_gate, grad_taps, grad_gain, grad_weight)


def solution(mesh):
    placed = (
        P("dp", "sp", None),
        P("dp", "sp", None),
        P("dp", "sp", None),
        P(None, "sp"),
        P(),
        P("dp", None),
    )
    return jax.shard_map(
        body,
        mesh=mesh,
        in_specs=placed,
        out_specs=(P("dp", "sp", None), P("dp", "sp", None), P(None, "sp"), P(), P("dp", None)),
        check_vma=False,
    )
```

profile of v0, /device:TPU:0, one launch (start us, length us, event | category | flops | bytes accessed | tf_op | source)
XLA Modules:
  0.0 395.5 jit_solution(13518251392995277205)
XLA Ops:
  7.9 1.5 copy.56
  9.4 1.9 copy.57
  11.9 12.9 %copy.90 = bf16[1,256,2048]{1,0,2:T(2,128)(2,1)} copy(bf16[1,256,2048]{1,2,0:T(8,128)(2,1)S(1)} %fusion.1) | data formatting | bytes 2097152 | tf_op jit(solution)/shard_map/convert_element_type | solution.py:13
  25.3 11.6 %reduce.17 = bf16[2048,256]{1,0:T(8,128)(2,1)S(1)} reduce(bf16[2048,1,256]{2,1,0:T(2,128)(2,1)} %bitcast.178, bf16[]{:T(256)} %broadcast.201), dimensions={1}, to_apply=%bitcast.161.reduce_sub_computation | reduce | bytes 2097154
  37.0 1.6 reshape.389
  38.6 5.4 %all-to-all-start = ((bf16[4,2,65536]{2,1,0:T(2,128)(2,1)}), bf16[4,2,65536]{2,1,0:T(2,128)(2,1)}, u32[]{:S(2)}, u32[]{:S(2)}) async-start(bf16[4,2,65536]{2,1,0:T(2,128)(2,1)} %reshape.389), calls=%async_computation | async-start | bytes 2097152 | tf_op jit(solution)/shard_map/all_to_all | solution.py:14
  44.1 14.2 %all-to-all-done = bf16[4,2,65536]{2,1,0:T(2,128)(2,1)} async-done(((bf16[4,2,65536]{2,1,0:T(2,128)(2,1)}), bf16[4,2,65536]{2,1,0:T(2,128)(2,1)}, u32[]{:S(2)}, u32[]{:S(2)}) %all-to-all-start) | async-done | bytes 1048608 | tf_op jit(solution)/shard_map/all_to_all | solution.py:14
  58.3 2.6 reshape.390
  60.9 1.6 copy_convert_fusion.2
  63.0 1.9 copy.60
  64.9 8.0 %add_convert_fusion.1 = bf16[1,1024,512]{2,1,0:T(8,128)(2,1)S(1)} fusion(f32[1,1024,512]{2,1,0:T(8,128)S(1)} %bitcast.163, f32[512]{0:T(512)S(1)} %bitcast.207, f32[512]{0:T(512)S(1)} %bitcast.209, f32[512]{0:T(512)S(1)} %bitcast.213, f32[512]{0:T(512)S(1)} %bitcast.215, f32[512]{0:T(512)S(1)} %bitcast.217, f32[512]{0:T(512)S(1)} %bitcast.219, ...), kind=kLoop, calls=%fused_computation.88 | loop fusion | flops 32505856 | bytes 3209216 | tf_op jit(solution)/shard_map/convert_element_type | solution.py:23
  72.9 2.9 copy.89
  75.8 8.1 %reduce.18 = bf16[1024,512]{1,0:T(8,128)(2,1)S(1)} reduce(bf16[1024,1,512]{2,1,0:T(2,128)(2,1)} %bitcast.180, bf16[]{:T(256)} %broadcast.201), dimensions={1}, to_apply=%bitcast.160.reduce_sub_computation | reduce | bytes 2097154
  83.9 2.0 reshape.391
  85.9 4.3 %all-to-all-start.1 = ((bf16[4,2,65536]{2,1,0:T(2,128)(2,1)}), bf16[4,2,65536]{2,1,0:T(2,128)(2,1)}, u32[]{:S(2)}, u32[]{:S(2)}) async-start(bf16[4,2,65536]{2,1,0:T(2,128)(2,1)} %reshape.391), calls=%async_computation.1 | async-start | bytes 2097152 | tf_op jit(solution)/shard_map/all_to_all | solution.py:22
  90.2 13.4 %all-to-all-done.1 = bf16[4,2,65536]{2,1,0:T(2,128)(2,1)} async-done(((bf16[4,2,65536]{2,1,0:T(2,128)(2,1)}), bf16[4,2,65536]{2,1,0:T(2,128)(2,1)}, u32[]{:S(2)}, u32[]{:S(2)}) %all-to-all-start.1) | async-done | bytes 1048608 | tf_op jit(solution)/shard_map/all_to_all | solution.py:22
  103.6 3.0 reshape.392
  108.0 1.8 copy_convert_fusion.1
  109.8 1.8 copy.63
  111.6 1.9 fusion.10
  113.5 1.8 fusion.32
  115.4 2.3 copy.71
  117.6 9.3 %convolution_bitcast_fusion = f32[2048,2048]{0,1:T(8,128)} fusion(bf16[256,2048]{0,1:T(8,128)(2,1)} %bitcast.186, bf16[1,256,2048]{2,1,0:T(8,128)(2,1)S(1)} %copy-done), kind=kOutput, calls=%fused_computation | convolution fusion | flops 2147483648 | bytes 18874368 | tf_op jit(solution)/shard_map/dot_general | solution.py:66
  126.9 1.4 copy.64
  129.2 5.7 %multiply_reduce_fusion = (f32[2048]{0:T(1024)S(1)}, f32[256]{0:T(256)S(1)}, f32[256]{0:T(256)S(1)}, f32[256,2048]{1,0:T(8,128)S(1)}) fusion(f32[256,2048]{1,0:T(8,128)S(1)} %bitcast.176, f32[256]{0:T(256)S(1)} %broadcast_multiply_fusion.2, f32[256]{0:T(256)S(1)} %add_rsqrt_fusion, f32[2048]{0:T(1024)S(1)} %copy-done.11, ...), kind=kOutput, calls=%fused_computation.20 | convolution fusion | flops 2156393984 | bytes 13651968 | tf_op jit(solution)/shard_map/dot_general | solution.py:34
  135.7 1.7 copy.65
  137.4 10.8 %reduce.19 = bf16[2048,256]{1,0:T(8,128)(2,1)S(1)} reduce(bf16[2048,1,256]{2,1,0:T(2,128)(2,1)S(1)} %bitcast.182, bf16[]{:T(256)} %broadcast.201), dimensions={1}, to_apply=%bitcast.148.reduce_sub_computation | reduce | bytes 2097154
  148.1 1.6 reshape.393
  149.8 3.5 all-to-all-start.2
  153.4 48.8 %psum.22 = f32[2048]{0:T(1024)} all-reduce(f32[2048]{0:T(1024)S(1)} %get-tuple-element.35), channel_id=1, replica_groups=mesh['sp'=4,'dp'=8] {'sp','dp'}, use_global_device_ids=true, to_apply=%region_39.40 | all-reduce | flops 2048 | bytes 16384 | tf_op jit(solution)/shard_map/psum | solution.py:63
  203.1 1.6 copy_convert_fusion
  205.1 1.9 copy.67
  207.1 8.0 %add_convert_fusion = bf16[1,1024,512]{2,1,0:T(8,128)(2,1)S(1)} fusion(f32[1,1024,512]{2,1,0:T(8,128)S(1)} %bitcast.162, f32[512]{0:T(512)S(1)} %bitcast.208, f32[512]{0:T(512)S(1)} %bitcast.210, f32[512]{0:T(512)S(1)} %bitcast.214, f32[512]{0:T(512)S(1)} %bitcast.216, f32[512]{0:T(512)S(1)} %bitcast.218, f32[512]{0:T(512)S(1)} %bitcast.220, ...), kind=kLoop, calls=%fused_computation.52 | loop fusion | flops 32505856 | bytes 3209216 | tf_op jit(solution)/shard_map/convert_element_type | solution.py:59
  215.0 81.4 %reduce-scatter.2.cloned.1.call-done = f32[256,2048]{0,1:T(8,128)} async-done(((f32[2048,2048]{0,1:T(8,128)}), f32[256,2048]{0,1:T(8,128)}) %reduce-scatter.2.cloned.1.call-update) | async-done | bytes 2097168 | tf_op jit(solution)/shard_map/reduce_scatter | solution.py:65
  296.5 17.9 %multiply_reduce_fusion.2 = (f32[512]{0:T(512)S(1)}, f32[512]{0:T(512)S(1)}, f32[512]{0:T(512)S(1)}, f32[512]{0:T(512)S(1)}, f32[512]{0:T(512)S(1)}, /*index=5*/...) fusion(f32[1,1024,512]{2,1,0:T(8,128)} %bitcast.164, ...), kind=kLoop, calls=%fused_computation.22 | loop fusion | flops 18865152 | bytes 4231168 | tf_op jit(solution)/shard_map/reduce_sum | solution.py:56
  314.4 2.9 copy.88
  317.4 8.0 %reduce.20 = bf16[1024,512]{1,0:T(8,128)(2,1)S(1)} reduce(bf16[1024,1,512]{2,1,0:T(2,128)(2,1)} %bitcast.179, bf16[]{:T(256)} %broadcast.201), dimensions={1}, to_apply=%bitcast.159.reduce_sub_computation | reduce | bytes 2097154
  325.4 2.0 reshape.395
  327.4 3.7 all-to-all-start.3
  331.1 2.6 multiply_reduce_fusion.1
  333.7 11.8 %multiply_reduce_fusion.3 = (f32[512]{0:T(512)S(1)}, f32[512]{0:T(512)S(1)}, f32[512]{0:T(512)S(1)}, f32[512]{0:T(512)S(1)}, f32[512]{0:T(512)S(1)}, /*index=5*/...) fusion(f32[1,1024,512]{2,1,0:T(8,128)} %bitcast.165, ...), kind=kLoop, calls=%fused_computation.23 | loop fusion | flops 12576768 | bytes 4218880 | tf_op jit(solution)/shard_map/reduce_sum | solution.py:56
  345.7 27.2 %psum.21 = f32[31,512]{1,0:T(8,128)} all-reduce(f32[31,512]{1,0:T(8,128)S(1)} %stack.127), channel_id=1, replica_groups=mesh['sp'=4,'dp'=8] {'dp'}, use_global_device_ids=true, to_apply=%region_37.38 | all-reduce | flops 15872 | bytes 126976 | tf_op jit(solution)/shard_map/psum | solution.py:57
  374.1 1.6 convert_bitcast_fusion
  375.7 3.0 copy.70
  378.8 3.4 fusion.4
  382.1 2.3 copy.72
  384.4 1.4 copy.73
  385.8 2.9 copy.74
  (53 shorter events, 8.3 us)
Async XLA Ops:
  7.2 110.5 %copy-start = (bf16[1,256,2048]{2,1,0:T(8,128)(2,1)S(1)}, bf16[1,256,2048]{2,1,0:T(8,128)(2,1)}, u32[]{:S(2)}) copy-start(bf16[1,256,2048]{2,1,0:T(8,128)(2,1)} %param.8) | copy-start | bytes 3145732
  7.2 122.0 %all-gather.2.cloned.1.call-start = ((), (), s32[]{:S(2)}) async-start(), calls=%async_computation.5 | async-start | bytes 9437184 | tf_op jit(solution)/shard_map/all_gather | solution.py:36
  9.4 2.5 copy-start.6
  11.3 13.5 %copy-start.8 = (bf16[1,256,2048]{1,2,0:T(8,128)(2,1)}, bf16[1,256,2048]{1,2,0:T(8,128)(2,1)S(1)}, u32[]{:S(2)}) copy-start(bf16[1,256,2048]{1,2,0:T(8,128)(2,1)S(1)} %copy.57) | copy-start | bytes 3145732
  37.0 7.1 %copy-start.10 = (f32[31,512]{1,0:T(8,128)S(1)}, f32[31,512]{1,0:T(8,128)}, u32[]{:S(2)}) copy-start(f32[31,512]{1,0:T(8,128)} %param.9) | copy-start | bytes 190468
  38.6 19.7 %all-to-all-start = ((bf16[4,2,65536]{2,1,0:T(2,128)(2,1)}), bf16[4,2,65536]{2,1,0:T(2,128)(2,1)}, u32[]{:S(2)}, u32[]{:S(2)}) async-start(bf16[4,2,65536]{2,1,0:T(2,128)(2,1)} %reshape.389), calls=%async_computation | async-start | bytes 2097152 | tf_op jit(solution)/shard_map/all_to_all | solution.py:14
  60.9 2.0 copy-start.3
  64.9 10.9 %copy-start.2 = (f32[1,4,256,512]{3,2,1,0:T(8,128)}, f32[1,4,256,512]{3,2,1,0:T(8,128)S(1)}, u32[]{:S(2)}) copy-start(f32[1,4,256,512]{3,2,1,0:T(8,128)S(1)} %copy.60) | copy-start | bytes 6291460
  83.9 6.3 %copy-start.11 = (f32[2048]{0:T(1024)S(1)}, f32[2048]{0:T(1024)}, u32[]{:S(2)}) copy-start(f32[2048]{0:T(1024)} %param.10) | copy-start | bytes 24580
  85.9 17.7 %all-to-all-start.1 = ((bf16[4,2,65536]{2,1,0:T(2,128)(2,1)}), bf16[4,2,65536]{2,1,0:T(2,128)(2,1)}, u32[]{:S(2)}, u32[]{:S(2)}) async-start(bf16[4,2,65536]{2,1,0:T(2,128)(2,1)} %reshape.391), calls=%async_computation.1 | async-start | bytes 2097152 | tf_op jit(solution)/shard_map/all_to_all | solution.py:22
  90.2 206.3 %reduce-scatter.2.cloned.1.call-start = ((), (), s32[]{:S(2)}) async-start(), calls=%async_computation.6 | async-start | bytes 18874368 | tf_op jit(solution)/shard_map/reduce_scatter | solution.py:65
  106.6 1.3 copy-start.5
  149.8 52.3 %all-to-all-start.2 = ((bf16[4,2,65536]{2,1,0:T(2,128)(2,1)}), bf16[4,2,65536]{2,1,0:T(2,128)(2,1)S(1)}, u32[]{:S(2)}, u32[]{:S(2)}) async-start(bf16[4,2,65536]{2,1,0:T(2,128)(2,1)} %reshape.393), calls=%async_computation.2 | async-start | bytes 2097152 | tf_op jit(solution)/shard_map/all_to_all | solution.py:47
  153.3 232.5 %all-reduce.4.cloned.1.call-start = ((), (), s32[]{:S(2)}) async-start(), calls=%async_computation.7 | async-start | bytes 4194304 | tf_op jit(solution)/shard_map/psum | solution.py:73
  203.1 2.0 copy-start.4
  327.4 45.5 %all-to-all-start.3 = ((bf16[4,2,65536]{2,1,0:T(2,128)(2,1)}), bf16[4,2,65536]{2,1,0:T(2,128)(2,1)S(1)}, u32[]{:S(2)}, u32[]{:S(2)}) async-start(bf16[4,2,65536]{2,1,0:T(2,128)(2,1)} %reshape.395), calls=%async_computation.3 | async-start | bytes 2097152 | tf_op jit(solution)/shard_map/all_to_all | solution.py:58
  375.7 3.0 copy-start.7
  375.7 3.0 copy-start.9
  384.4 4.3 %copy-start.1 = (bf16[1,256,2048]{2,1,0:T(8,128)(2,1)S(1)}, bf16[1,256,2048]{2,1,0:T(8,128)(2,1)}, u32[]{:S(2)}) copy-start(bf16[1,256,2048]{2,1,0:T(8,128)(2,1)} %param.8) | copy-start | bytes 3145732
Sparse Core Ops, SparseCore 0:
  9.6 84.7 all-gather.1
  127.1 169.3 reduce-scatter.1
  299.6 69.1 all-reduce.3
where the time goes:
time: 402 us; the launch traced here: 395 us
  waiting for transfers between devices  110 us (27%)
  other arithmetic  102 us (25%)
  blocking collectives  75.9 us (19%)
  local copies, waits for them, and re-layouts  61.5 us (15%)
  starting transfers between devices  16.9 us (4%)
  matrix products  15 us (4%)
  between operations  14.3 us (4%)
    reduce_scatter x1, waiting for transfers between devices, body(): lax.psum_scatter(lax.dot_general(columns, activated, (((0,), (0,)), ((),...  81.4 us
    psum x1, blocking collectives, body(): grad_gain = lax.psum(gain_part, ('sp', 'dp'))  48.8 us
    unnamed x4, other arithmetic  38.5 us
    reduce_sum x4, other arithmetic, body(): jnp.sum(grad_heads * padded[:, offset:offset + length], axis=(0, 1))  32.4 us
    unnamed x39, local copies, waits for them, and re-layouts  28.2 us
    psum x1, blocking collectives, body(): grad_taps = lax.psum(jnp.stack(tap_terms), 'dp')  27.2 us
    all_to_all x1, waiting for transfers between devices, body(): lax.all_to_all(glu, 'sp', split_axis=2, concat_axis=1, tiled=True)  14.2 us
    all_to_all x1, waiting for transfers between devices, body(): lax.all_to_all(conv_out.astype(jnp.bfloat16), 'sp', split_axis=1, concat_...  13.4 us
  transfers between devices with their start and end apart: 7, of which 3 were waited for; matrix products, arithmetic and copies ran while one was open for 44% of the time, Pallas kernels for 0%

commit v1 on v0

--- a/solution.py
+++ b/solution.py
@@ -60,7 +60,7 @@
     ).astype(jnp.float32)
     grad_value = (grad_tokens * sig_gate).astype(jnp.bfloat16)
     grad_gate = (grad_tokens * value_wide * sig_gate * (1.0 - sig_gate)).astype(jnp.bfloat16)
-    grad_gain = lax.psum(gain_part, ("sp", "dp"))
+    grad_gain = lax.psum(lax.psum(gain_part, axis_name="dp"), axis_name="sp")
     columns = upstream_rows
     owned = lax.psum_scatter(
         lax.dot_general(

time: 402 us -> 449 us (1.12)
  waiting for transfers between devices: 110 us -> 212 us
  blocking collectives: 75.9 us -> 27 us
  other arithmetic: 102 us -> 87.9 us
  starting transfers between devices: 16.9 us -> 24.8 us
    psum x2 -> x1, blocking collectives: 75.9 us -> 10.9 us  [body(): grad_gain = lax.psum(lax.psum(gain_part, axis_name='dp'), axis_name='sp')]
    psum x1, waiting for transfers between devices: 0.01 us -> 50.9 us  [body(): grad_weight = lax.psum(owned, 'sp')]
    psum x0 -> x1, waiting for transfers between devices: none -> 29.5 us  [body(): grad_taps = lax.psum(jnp.stack(tap_terms), 'dp')]
    reduce_scatter x1, waiting for transfers between devices: 81.4 us -> 103 us  [body(): lax.psum_scatter(lax.dot_general(columns, activated, (((0,), (0,)), ((),...]
    all_to_all x0 -> x1, blocking collectives: none -> 16.1 us  [body(): lax.all_to_all(grad_conv_out.astype(jnp.bfloat16), 'sp', split_axis=2, co...]
    reduce_sum x4, other arithmetic: 32.4 us -> 19.5 us  [body(): jnp.sum(grad_heads * padded[:, offset:offset + length], axis=(0, 1))]
    all_to_all x1, starting transfers between devices: 5.38 us -> 16.2 us  [body(): lax.all_to_all(glu, 'sp', split_axis=2, concat_axis=1, tiled=True)]
    unnamed x39 -> x44, local copies, waits for them, and re-layouts: 28.2 us -> 27.1 us
  transfers between devices with their start and end apart: 7 -> 7, of which waited for: 3 -> 5; matrix products, arithmetic and copies ran while one was open for 44% -> 36% of each run, Pallas kernels for 0% -> 0%
where the time goes in v1:
time: 449 us; the launch traced here: 443 us
  waiting for transfers between devices  212 us (47%)
  other arithmetic  87.9 us (20%)
  local copies, waits for them, and re-layouts  61.5 us (14%)
  blocking collectives  27 us (6%)
  starting transfers between devices  24.8 us (6%)
  matrix products  15.6 us (3%)
  between operations  14.3 us (3%)
    reduce_scatter x1, waiting for transfers between devices, body(): lax.psum_scatter(lax.dot_general(columns, activated, (((0,), (0,)), ((),...  103 us
    psum x1, waiting for transfers between devices, body(): grad_weight = lax.psum(owned, 'sp')  50.9 us
    unnamed x4, other arithmetic  37.3 us
    psum x1, waiting for transfers between devices, body(): grad_taps = lax.psum(jnp.stack(tap_terms), 'dp')  29.5 us
    unnamed x44, local copies, waits for them, and re-layouts  27.1 us
    reduce_sum x4, other arithmetic, body(): jnp.sum(grad_heads * padded[:, offset:offset + length], axis=(0, 1))  19.5 us
    all_to_all x1, starting transfers between devices, body(): lax.all_to_all(glu, 'sp', split_axis=2, concat_axis=1, tiled=True)  16.2 us
    all_to_all x1, blocking collectives, body(): lax.all_to_all(grad_conv_out.astype(jnp.bfloat16), 'sp', split_axis=2, co...  16.1 us
  transfers between devices with their start and end apart: 7, of which 5 were waited for; matrix products, arithmetic and copies ran while one was open for 36% of the time, Pallas kernels for 0%

profile of v1, /device:TPU:0, one launch (start us, length us, event | category | flops | bytes accessed | tf_op | source)
XLA Modules:
  0.0 443.0 jit_solution(5670113685934083878)
XLA Ops:
  7.9 1.5 copy.56
  9.4 1.9 copy.57
  11.9 12.9 %copy.90 = bf16[1,256,2048]{1,0,2:T(2,128)(2,1)} copy(bf16[1,256,2048]{1,2,0:T(8,128)(2,1)S(1)} %fusion.1) | data formatting | bytes 2097152 | tf_op jit(solution)/shard_map/convert_element_type | solution.py:13
  25.4 11.6 %reduce.17 = bf16[2048,256]{1,0:T(8,128)(2,1)S(1)} reduce(bf16[2048,1,256]{2,1,0:T(2,128)(2,1)} %bitcast.178, bf16[]{:T(256)} %broadcast.201), dimensions={1}, to_apply=%bitcast.161.reduce_sub_computation | reduce | bytes 2097154
  37.0 1.6 reshape.389
  38.7 16.2 %all-to-all-start = ((bf16[4,2,65536]{2,1,0:T(2,128)(2,1)}), bf16[4,2,65536]{2,1,0:T(2,128)(2,1)}, u32[]{:S(2)}, u32[]{:S(2)}) async-start(bf16[4,2,65536]{2,1,0:T(2,128)(2,1)} %reshape.389), calls=%async_computation | async-start | bytes 2097152 | tf_op jit(solution)/shard_map/all_to_all | solution.py:14
  55.0 14.5 %all-to-all-done = bf16[4,2,65536]{2,1,0:T(2,128)(2,1)} async-done(((bf16[4,2,65536]{2,1,0:T(2,128)(2,1)}), bf16[4,2,65536]{2,1,0:T(2,128)(2,1)}, u32[]{:S(2)}, u32[]{:S(2)}) %all-to-all-start) | async-done | bytes 1048608 | tf_op jit(solution)/shard_map/all_to_all | solution.py:14
  69.5 2.6 reshape.390
  72.2 1.6 copy_convert_fusion.2
  74.2 1.9 copy.60
  76.1 8.0 %add_convert_fusion.1 = bf16[1,1024,512]{2,1,0:T(8,128)(2,1)S(1)} fusion(f32[1,1024,512]{2,1,0:T(8,128)S(1)} %bitcast.163, f32[512]{0:T(512)S(1)} %bitcast.207, f32[512]{0:T(512)S(1)} %bitcast.209, f32[512]{0:T(512)S(1)} %bitcast.213, f32[512]{0:T(512)S(1)} %bitcast.215, f32[512]{0:T(512)S(1)} %bitcast.217, f32[512]{0:T(512)S(1)} %bitcast.219, ...), kind=kLoop, calls=%fused_computation.88 | loop fusion | flops 32505856 | bytes 3209216 | tf_op jit(solution)/shard_map/convert_element_type | solution.py:23
  84.1 2.9 copy.89
  87.0 8.1 %reduce.18 = bf16[1024,512]{1,0:T(8,128)(2,1)S(1)} reduce(bf16[1024,1,512]{2,1,0:T(2,128)(2,1)} %bitcast.180, bf16[]{:T(256)} %broadcast.201), dimensions={1}, to_apply=%bitcast.160.reduce_sub_computation | reduce | bytes 2097154
  95.1 2.0 reshape.391
  97.1 4.3 all-to-all-start.1
  101.4 13.4 %all-to-all-done.1 = bf16[4,2,65536]{2,1,0:T(2,128)(2,1)} async-done(((bf16[4,2,65536]{2,1,0:T(2,128)(2,1)}), bf16[4,2,65536]{2,1,0:T(2,128)(2,1)}, u32[]{:S(2)}, u32[]{:S(2)}) %all-to-all-start.1) | async-done | bytes 1048608 | tf_op jit(solution)/shard_map/all_to_all | solution.py:22
  114.8 2.6 reshape.392
  118.8 1.8 copy_convert_fusion.1
  120.6 1.8 copy.63
  122.4 1.9 fusion.10
  124.3 1.8 fusion.32
  126.2 2.3 copy.71
  128.4 9.3 %convolution_bitcast_fusion = f32[2048,2048]{0,1:T(8,128)} fusion(bf16[256,2048]{0,1:T(8,128)(2,1)} %bitcast.186, bf16[1,256,2048]{2,1,0:T(8,128)(2,1)S(1)} %copy-done), kind=kOutput, calls=%fused_computation | convolution fusion | flops 2147483648 | bytes 18874368 | tf_op jit(solution)/shard_map/dot_general | solution.py:66
  140.4 6.4 %multiply_reduce_fusion = (f32[2048]{0:T(1024)}, f32[256]{0:T(256)S(1)}, f32[256]{0:T(256)S(1)}, f32[256,2048]{1,0:T(8,128)S(1)}) fusion(f32[256,2048]{1,0:T(8,128)S(1)} %bitcast.176, f32[256]{0:T(256)S(1)} %broadcast_multiply_fusion.2, f32[256]{0:T(256)S(1)} %add_rsqrt_fusion, f32[2048]{0:T(1024)S(1)} %copy-done.13, ...), kind=kOutput, calls=%fused_computation.20 | convolution fusion | flops 2156393984 | bytes 13651968 | tf_op jit(solution)/shard_map/dot_general | solution.py:34
  147.5 1.7 copy.65
  149.2 10.6 %reduce.19 = bf16[2048,256]{1,0:T(8,128)(2,1)S(1)} reduce(bf16[2048,1,256]{2,1,0:T(2,128)(2,1)S(1)} %bitcast.182, bf16[]{:T(256)} %broadcast.201), dimensions={1}, to_apply=%bitcast.148.reduce_sub_computation | reduce | bytes 2097154
  160.1 16.1 %all_to_all.16 = bf16[4,2,65536]{2,1,0:T(2,128)(2,1)S(1)} all-to-all(bf16[4,2,65536]{2,1,0:T(2,128)(2,1)S(1)} %reshape.393), channel_id=1, replica_groups=mesh['sp'=4,'dp'=8] {'sp'}, dimensions={0} | all-to-all | bytes 2097152 | tf_op jit(solution)/shard_map/all_to_all | solution.py:47
  177.2 1.6 copy_convert_fusion
  179.1 2.0 copy.67
  181.1 2.6 multiply_reduce_fusion.1
  183.8 11.8 %multiply_reduce_fusion.3 = (f32[512]{0:T(512)S(1)}, f32[512]{0:T(512)S(1)}, f32[512]{0:T(512)S(1)}, f32[512]{0:T(512)S(1)}, f32[512]{0:T(512)S(1)}, /*index=5*/...) fusion(f32[1,1024,512]{2,1,0:T(8,128)} %bitcast.164, ...), kind=kLoop, calls=%fused_computation.23 | loop fusion | flops 12576768 | bytes 4218880 | tf_op jit(solution)/shard_map/reduce_sum | solution.py:56
  195.6 5.0 %multiply_reduce_fusion.2 = (f32[512]{0:T(512)S(1)}, f32[512]{0:T(512)S(1)}, f32[512]{0:T(512)S(1)}, f32[512]{0:T(512)S(1)}, f32[512]{0:T(512)S(1)}, /*index=5*/...) fusion(f32[1,1024,512]{2,1,0:T(8,128)S(1)} %bitcast.165, ...), kind=kLoop, calls=%fused_computation.22 | loop fusion | flops 18865152 | bytes 4231168 | tf_op jit(solution)/shard_map/reduce_sum | solution.py:56
  200.6 2.5 stack.127
  203.4 102.7 %reduce-scatter.2.cloned.1.call-done = f32[256,2048]{0,1:T(8,128)} async-done(((f32[2048,2048]{0,1:T(8,128)}), f32[256,2048]{0,1:T(8,128)}) %reduce-scatter.2.cloned.1.call-update) | async-done | bytes 2097168 | tf_op jit(solution)/shard_map/reduce_scatter | solution.py:65
  306.2 8.0 %add_convert_fusion = bf16[1,1024,512]{2,1,0:T(8,128)(2,1)S(1)} fusion(f32[1,1024,512]{2,1,0:T(8,128)S(1)} %bitcast.162, f32[512]{0:T(512)S(1)} %bitcast.208, f32[512]{0:T(512)S(1)} %bitcast.210, f32[512]{0:T(512)S(1)} %bitcast.214, f32[512]{0:T(512)S(1)} %bitcast.216, f32[512]{0:T(512)S(1)} %bitcast.218, f32[512]{0:T(512)S(1)} %bitcast.220, ...), kind=kLoop, calls=%fused_computation.52 | loop fusion | flops 32505856 | bytes 3209216 | tf_op jit(solution)/shard_map/convert_element_type | solution.py:59
  314.1 1.6 copy.88
  315.8 7.0 %reduce.20 = bf16[1024,512]{1,0:T(8,128)(2,1)S(1)} reduce(bf16[1024,1,512]{2,1,0:T(2,128)(2,1)S(1)} %bitcast.179, bf16[]{:T(256)} %broadcast.201), dimensions={1}, to_apply=%bitcast.159.reduce_sub_computation | reduce | bytes 2097154
  322.8 2.0 reshape.395
  324.8 3.6 all-to-all-start.3
  328.4 29.5 %all-reduce.8.cloned.1.call-done = (f32[31,512]{1,0:T(8,128)}, f32[2048]{0:T(1024)}) async-done(((f32[31,512]{1,0:T(8,128)}, f32[2048]{0:T(1024)}), (f32[31,512]{1,0:T(8,128)}, f32[2048]{0:T(1024)})) %all-reduce.8.cloned.1.call-update) | async-done | bytes 71696 | tf_op jit(solution)/shard_map/psum | solution.py:57
  357.9 10.9 %psum.30 = f32[2048]{0:T(1024)} all-reduce(f32[2048]{0:T(1024)} %get-tuple-element.69), channel_id=1, replica_groups=mesh['sp'=4,'dp'=8] {'sp'}, use_global_device_ids=true, to_apply=%region_40.41 | all-reduce | flops 2048 | bytes 16384 | tf_op jit(solution)/shard_map/psum | solution.py:63
  370.0 1.6 convert_bitcast_fusion
  371.7 3.0 copy.70
  374.7 3.4 fusion.4
  378.1 2.3 copy.72
  380.4 1.4 copy.73
  381.8 50.9 %all-reduce.6.cloned.1.call-done = f32[256,2048]{0,1:T(8,128)} async-done(((f32[256,2048]{0,1:T(8,128)}), f32[256,2048]{0,1:T(8,128)}) %all-reduce.6.cloned.1.call-update) | async-done | bytes 2097168 | tf_op jit(solution)/shard_map/psum | solution.py:73
  432.7 2.9 copy.74
  (59 shorter events, 11.1 us)
Async XLA Ops:
  7.2 121.2 %copy-start = (bf16[1,256,2048]{2,1,0:T(8,128)(2,1)S(1)}, bf16[1,256,2048]{2,1,0:T(8,128)(2,1)}, u32[]{:S(2)}) copy-start(bf16[1,256,2048]{2,1,0:T(8,128)(2,1)} %param.8) | copy-start | bytes 3145732
  7.2 133.3 %all-gather.2.cloned.1.call-start = ((), (), s32[]{:S(2)}) async-start(), calls=%async_computation.5 | async-start | bytes 9437184 | tf_op jit(solution)/shard_map/all_gather | solution.py:36
  9.4 2.5 copy-start.7
  11.3 13.5 %copy-start.9 = (bf16[1,256,2048]{1,2,0:T(8,128)(2,1)}, bf16[1,256,2048]{1,2,0:T(8,128)(2,1)S(1)}, u32[]{:S(2)}) copy-start(bf16[1,256,2048]{1,2,0:T(8,128)(2,1)S(1)} %copy.57) | copy-start | bytes 3145732
  37.0 17.9 %copy-start.12 = (f32[31,512]{1,0:T(8,128)S(1)}, f32[31,512]{1,0:T(8,128)}, u32[]{:S(2)}) copy-start(f32[31,512]{1,0:T(8,128)} %param.9) | copy-start | bytes 190468
  38.7 30.8 %all-to-all-start = ((bf16[4,2,65536]{2,1,0:T(2,128)(2,1)}), bf16[4,2,65536]{2,1,0:T(2,128)(2,1)}, u32[]{:S(2)}, u32[]{:S(2)}) async-start(bf16[4,2,65536]{2,1,0:T(2,128)(2,1)} %reshape.389), calls=%async_computation | async-start | bytes 2097152 | tf_op jit(solution)/shard_map/all_to_all | solution.py:14
  72.1 2.0 copy-start.4
  76.1 10.9 %copy-start.2 = (f32[1,4,256,512]{3,2,1,0:T(8,128)}, f32[1,4,256,512]{3,2,1,0:T(8,128)S(1)}, u32[]{:S(2)}) copy-start(f32[1,4,256,512]{3,2,1,0:T(8,128)S(1)} %copy.60) | copy-start | bytes 6291460
  95.1 6.3 %copy-start.13 = (f32[2048]{0:T(1024)S(1)}, f32[2048]{0:T(1024)}, u32[]{:S(2)}) copy-start(f32[2048]{0:T(1024)} %param.10) | copy-start | bytes 24580
  97.1 17.7 %all-to-all-start.1 = ((bf16[4,2,65536]{2,1,0:T(2,128)(2,1)}), bf16[4,2,65536]{2,1,0:T(2,128)(2,1)}, u32[]{:S(2)}, u32[]{:S(2)}) async-start(bf16[4,2,65536]{2,1,0:T(2,128)(2,1)} %reshape.391), calls=%async_computation.1 | async-start | bytes 2097152 | tf_op jit(solution)/shard_map/all_to_all | solution.py:22
  101.4 204.8 %reduce-scatter.2.cloned.1.call-start = ((), (), s32[]{:S(2)}) async-start(), calls=%async_computation.6 | async-start | bytes 18874368 | tf_op jit(solution)/shard_map/reduce_scatter | solution.py:65
  117.4 1.3 copy-start.6
  137.7 220.2 %all-reduce.8.cloned.1.call-start = ((), (), s32[]{:S(2)}) async-start(), calls=%async_computation.8 | async-start | bytes 147456 | tf_op jit(solution)/shard_map/psum | solution.py:57
  177.2 2.0 copy-start.5
  183.8 11.8 %copy-start.3 = (f32[1,4,256,512]{3,2,1,0:T(8,128)S(1)}, f32[1,4,256,512]{3,2,1,0:T(8,128)}, u32[]{:S(2)}) copy-start(f32[1,4,256,512]{3,2,1,0:T(8,128)} %copy-done.2) | copy-start | bytes 6291460
  203.2 229.6 %all-reduce.6.cloned.1.call-start = ((), (), s32[]{:S(2)}) async-start(), calls=%async_computation.7 | async-start | bytes 4194304 | tf_op jit(solution)/shard_map/psum | solution.py:73
  324.8 44.0 %all-to-all-start.3 = ((bf16[4,2,65536]{2,1,0:T(2,128)(2,1)}), bf16[4,2,65536]{2,1,0:T(2,128)(2,1)S(1)}, u32[]{:S(2)}, u32[]{:S(2)}) async-start(bf16[4,2,65536]{2,1,0:T(2,128)(2,1)} %reshape.395), calls=%async_computation.3 | async-start | bytes 2097152 | tf_op jit(solution)/shard_map/all_to_all | solution.py:58
  371.7 3.0 copy-start.8
  371.7 3.0 copy-start.10
  380.4 55.9 %copy-start.1 = (bf16[1,256,2048]{2,1,0:T(8,128)(2,1)S(1)}, bf16[1,256,2048]{2,1,0:T(8,128)(2,1)}, u32[]{:S(2)}) copy-start(bf16[1,256,2048]{2,1,0:T(8,128)(2,1)} %param.8) | copy-start | bytes 3145732
  381.8 53.8 %copy-start.11 = (f32[31,512]{1,0:T(8,128)S(1)}, f32[31,512]{1,0:T(8,128)}, u32[]{:S(2)}) copy-start(f32[31,512]{1,0:T(8,128)} %get-tuple-element.108) | copy-start | bytes 190468
Sparse Core Ops, SparseCore 0:
  9.6 84.7 all-gather.1
  137.8 168.2 reduce-scatter.1
  309.1 48.7 all-reduce.7
  360.9 71.8 all-reduce.5
